TPU v7x, 32 devices: a whole 2x2x4 slice. The times are simulated.
32 devices in a mesh: grp: 2 (over y), sp: 4 (over z), dp: 4 (over x, core).
Axes of the slice: x: 2, y: 2, z: 4, core: 2. Of those that a mesh axis runs over, the one named last changes fastest.
Arguments:
- tokens: bfloat16 [8, 512, 2048], P(('grp', 'dp'), 'sp'), parts along dimension 0, may hold values from -6 to 6
- forget_offset: float32 [8, 512], P(('grp', 'dp'), 'sp'), parts along dimension 0, may hold values from -1.2 to 1.2, as said below
- q_weight: bfloat16 [2048, 2048], P(None, 'dp'), may hold values from -0.125 to 0.125
- k_weight: bfloat16 [2048, 512], P(None, 'dp'), may hold values from -0.125 to 0.125
- v_weight: bfloat16 [2048, 512], P(None, 'dp'), may hold values from -0.125 to 0.125
- forget_weight: bfloat16 [2048, 16], replicated, may hold values from -0.125 to 0.125
- forget_bias: float32 [16], replicated, may hold values from 3 to 12
- score_gain: float32 [16], replicated, may hold values from 0.5 to 80
- out_gain: float32 [2048], replicated, may hold values from 0.1 to 1.9
Outputs:
- attended: bfloat16 [8, 512, 2048], P(('grp', 'dp'), 'sp'), parts along dimension 0
There are 2 independent parts, one for each index of `grp`. A program takes and returns all parts, laid end to end along the dimension named above; an argument that names none is the same for every part. Nothing has to cross between parts.
Inputs may be any that keep to these rules, and one draw needn't show every extreme that they name: `forget_offset`: constant over aligned spans of 64 positions.
All inputs are finite; a program needn't handle non-finite values.
Results may differ from a plain program's by a relative error of at most 0.0085.
The roundings to bfloat16 on the way count: a program that leaves them out, or rounds other values in their place, can miss the bound.
Values may be sent and summed in bfloat16 or wider, within the bound.
A program may use at most 128 MiB of HBM per device.

v0:
```python
import jax
import jax.numpy as jnp
from jax import lax
from jax.sharding import PartitionSpec as P

NEG = -1e30
QK_FLOOR = 0.1
OUT_FLOOR = 0.001


def head_norm(vectors, floor):
    return vectors * lax.rsqrt(jnp.mean(vectors * vectors, axis=-1, keepdims=True) + floor)


def local(
    tokens,
    forget_offset,
    q_weight,
    k_weight,
    v_weight,
    forget_weight,
    forget_bias,
    score_gain,
    out_gain,
):
    own_rows = tokens[0]
    tok_count = own_rows.shape[0]
    head_count = forget_bias.shape[0]
    head_dim = out_gain.shape[0] // head_count
    kv_heads = k_weight.shape[1] * lax.axis_size("dp") // head_dim
    spread = lax.axis_size("sp")
    local_heads = head_count // spread
    local_kv = max(1, kv_heads // spread)
    group_size = local_heads // local_kv
    everyone = lax.all_gather(tokens, "dp", axis=0, tiled=True)
    seq_count = everyone.shape[0]
    flat_rows = everyone.reshape(seq_count * tok_count, everyone.shape[2])
    query_cols = (
        jnp.dot(flat_rows, q_weight, preferred_element_type=jnp.float32)
        .astype(jnp.bfloat16)
        .reshape(seq_count, tok_count, -1)
    )
    key_cols = (
        jnp.dot(flat_rows, k_weight, preferred_element_type=jnp.float32)
        .astype(jnp.bfloat16)
        .reshape(seq_count, tok_count, -1)
    )
    value_cols = (
        jnp.dot(flat_rows, v_weight, preferred_element_type=jnp.float32)
        .astype(jnp.bfloat16)
        .reshape(seq_count, tok_count, -1)
    )
    query_mine, key_mine, value_mine = (
        lax.all_to_all(query_cols, "dp", split_axis=0, concat_axis=2, tiled=True),
        lax.all_to_all(key_cols, "dp", split_axis=0, concat_axis=2, tiled=True),
        lax.all_to_all(value_cols, "dp", split_axis=0, concat_axis=2, tiled=True),
    )
    queries = query_mine[0]
    keys_proj = key_mine[0]
    values_proj = value_mine[0]
    forget_input = (
        jnp.dot(own_rows, forget_weight, preferred_element_type=jnp.float32)
        + forget_offset[0][:, None]
    ).astype(jnp.bfloat16)
    query_send = queries.reshape(tok_count, spread, local_heads, head_dim)
    forget_send = forget_input.reshape(tok_count, spread, local_heads)
    if kv_heads >= spread:
        key_send = keys_proj.reshape(tok_count, spread, local_kv, head_dim)
        value_send = values_proj.reshape(tok_count, spread, local_kv, head_dim)
    else:
        copies = spread // kv_heads
        key_send = jnp.broadcast_to(
            keys_proj.reshape(tok_count, kv_heads, 1, head_dim),
            (tok_count, kv_heads, copies, head_dim),
        ).reshape(tok_count, spread, 1, head_dim)
        value_send = jnp.broadcast_to(
            values_proj.reshape(tok_count, kv_heads, 1, head_dim),
            (tok_count, kv_heads, copies, head_dim),
        ).reshape(tok_count, spread, 1, head_dim)
    query_head, forget_head, key_head, value_head = (
        lax.all_to_all(query_send, "sp", split_axis=1, concat_axis=0, tiled=True),
        lax.all_to_all(forget_send, "sp", split_axis=1, concat_axis=0, tiled=True),
        lax.all_to_all(key_send, "sp", split_axis=1, concat_axis=0, tiled=True),
        lax.all_to_all(value_send, "sp", split_axis=1, concat_axis=0, tiled=True),
    )
    length = query_head.shape[0]
    first_head = lax.axis_index("sp") * local_heads
    bias_local = lax.dynamic_slice_in_dim(forget_bias, first_head, local_heads, 0)
    gain_local = lax.dynamic_slice_in_dim(score_gain, first_head, local_heads, 0)
    norm_local = lax.dynamic_slice_in_dim(
        out_gain, first_head * head_dim, local_heads * head_dim, 0
    )
    log_gate = jax.nn.log_sigmoid(
        forget_head.reshape(length, local_heads).astype(jnp.float32) + bias_local[None, :]
    )
    cumulative = jnp.cumsum(log_gate, axis=0).reshape(length, local_kv, group_size)
    query_unit = head_norm(query_head.astype(jnp.float32), QK_FLOOR).astype(jnp.bfloat16)
    key_unit = head_norm(
        key_head.reshape(length, local_kv, head_dim).astype(jnp.float32), QK_FLOOR
    ).astype(jnp.bfloat16)
    value_heads = value_head.reshape(length, local_kv, head_dim)
    factor = (gain_local * head_dim ** (-0.5)).reshape(local_kv, group_size)
    out_gains = norm_local.reshape(local_kv, group_size, head_dim)
    key_totals = jnp.transpose(cumulative, (1, 2, 0))
    span_rows = 512
    positions = jnp.arange(length, dtype=jnp.int32)

    def attend_block(block_index):
        first = block_index * span_rows
        query_block = lax.dynamic_slice_in_dim(query_unit, first, span_rows, 0)
        query_totals = lax.dynamic_slice_in_dim(cumulative, first, span_rows, 0)
        scores = jnp.einsum(
            "qkgd,skd->kgqs", query_block, key_unit, preferred_element_type=jnp.float32
        )
        scores = (
            scores * factor[:, :, None, None]
            + jnp.transpose(query_totals, (1, 2, 0))[..., None]
            - key_totals[:, :, None, :]
        )
        allowed = positions[None, :] <= (first + jnp.arange(span_rows, dtype=jnp.int32))[:, None]
        scores = jnp.where(allowed[None, None], scores, NEG)
        row_peak = jnp.max(scores, axis=-1, keepdims=True)
        exponent = jnp.exp(scores - row_peak)
        weights = (exponent / jnp.sum(exponent, axis=-1, keepdims=True)).astype(jnp.bfloat16)
        mixed = jnp.einsum(
            "kgqs,skd->qkgd", weights, value_heads, preferred_element_type=jnp.float32
        )
        return (head_norm(mixed, OUT_FLOOR) * out_gains).astype(jnp.bfloat16)

    outputs = lax.map(attend_block, jnp.arange(length // span_rows, dtype=jnp.int32))
    outputs = outputs.reshape(length, local_heads, head_dim)
    back_rows = lax.all_to_all(outputs, "sp", split_axis=0, concat_axis=1, tiled=True)
    return back_rows.reshape(1, tok_count, head_count * head_dim)


def solution(mesh):
    in_specs = (
        P(("grp", "dp"), "sp", None),
        P(("grp", "dp"), "sp"),
        P(None, "dp"),
        P(None, "dp"),
        P(None, "dp"),
        P(),
        P(),
        P(),
        P(),
    )
    out_specs = P(("grp", "dp"), "sp", None)
    return jax.shard_map(local, mesh=mesh, in_specs=in_specs, out_specs=out_specs, check_vma=False)
```

profile of v0, /device:TPU:0, one launch (start us, length us, event | category | flops | bytes accessed | tf_op | source)
XLA Modules:
  0.0 133.0 jit_solution(4874085769551353659)
XLA Ops:
  7.3 2.0 %fusion.10 = bf16[128,16]{0,1:T(8,128)(2,1)} fusion(bf16[2048,16]{0,1:T(8,128)(2,1)} %param.14, bf16[1,128,2048]{2,1,0:T(8,128)(2,1)} %param.9, f32[128]{0:T(128)} %bitcast.174), kind=kOutput, calls=%fused_computation.16 | convolution fusion | flops 8392704 | bytes 594432 | tf_op jit(solution)/shard_map/dot_general | solution.py:62
  9.2 6.3 %all-to-all-start.6 = ((bf16[128,4,4]{0,2,1:T(4,128)(2,1)}), bf16[128,4,4]{0,2,1:T(4,128)(2,1)S(1)}, u32[]{:S(2)}, u32[]{:S(2)}) async-start(bf16[128,4,4]{0,2,1:T(4,128)(2,1)} %bitcast.32), calls=%async_computation.6 | async-start | bytes 8192 | tf_op jit(solution)/shard_map/all_to_all | solution.py:82
  15.6 18.6 %all-gather.2.cloned.1.call-done = bf16[4,128,2048]{2,1,0:T(8,128)(2,1)} async-done(((bf16[1,128,2048]{2,1,0:T(8,128)(2,1)}), bf16[4,128,2048]{2,1,0:T(8,128)(2,1)}) %all-gather.2.cloned.1.call-update) | async-done | bytes 2097168 | tf_op jit(solution)/shard_map/all_gather | solution.py:35
  34.2 3.0 %convolution_convert_fusion.2 = bf16[512,128]{1,0:T(8,128)(2,1)} fusion(bf16[512,2048]{1,0:T(8,128)(2,1)} %bitcast.161, bf16[2048,128]{1,0:T(8,128)(2,1)} %param.13), kind=kOutput, calls=%fused_computation.14 | convolution fusion | flops 268500992 | bytes 2752512 | tf_op jit(solution)/shard_map/dot_general | solution.py:49
  37.3 4.0 %all-to-all-start = ((bf16[4,128,128]{2,1,0:T(8,128)(2,1)}), bf16[4,128,128]{2,1,0:T(8,128)(2,1)}, u32[]{:S(2)}, u32[]{:S(2)}) async-start(bf16[4,128,128]{2,1,0:T(8,128)(2,1)} %bitcast.1), calls=%async_computation | async-start | bytes 262144 | tf_op jit(solution)/shard_map/all_to_all | solution.py:56
  41.2 3.0 %convolution_convert_fusion.1 = bf16[512,128]{1,0:T(8,128)(2,1)} fusion(bf16[512,2048]{1,0:T(8,128)(2,1)} %bitcast.162, bf16[2048,128]{1,0:T(8,128)(2,1)S(1)} %copy-done.2), kind=kOutput, calls=%fused_computation.13 | convolution fusion | flops 268500992 | bytes 2752512 | tf_op jit(solution)/shard_map/dot_general | solution.py:44
  44.2 1.7 %all-to-all-done = bf16[4,128,128]{2,1,0:T(8,128)(2,1)} async-done(((bf16[4,128,128]{2,1,0:T(8,128)(2,1)}), bf16[4,128,128]{2,1,0:T(8,128)(2,1)}, u32[]{:S(2)}, u32[]{:S(2)}) %all-to-all-start) | async-done | bytes 131104 | tf_op jit(solution)/shard_map/all_to_all | solution.py:56
  45.9 4.0 %all-to-all-start.2 = ((bf16[4,128,128]{2,1,0:T(8,128)(2,1)}), bf16[4,128,128]{2,1,0:T(8,128)(2,1)}, u32[]{:S(2)}, u32[]{:S(2)}) async-start(bf16[4,128,128]{2,1,0:T(8,128)(2,1)} %bitcast.9), calls=%async_computation.2 | async-start | bytes 262144 | tf_op jit(solution)/shard_map/all_to_all | solution.py:55
  49.9 2.8 %convolution_convert_fusion = bf16[512,512]{1,0:T(8,128)(2,1)S(1)} fusion(bf16[512,2048]{1,0:T(8,128)(2,1)} %bitcast.163, bf16[2048,512]{1,0:T(8,128)(2,1)S(1)} %copy-done), kind=kOutput, calls=%fused_computation.12 | convolution fusion | flops 1074003968 | bytes 4718592 | tf_op jit(solution)/shard_map/dot_general | solution.py:39
  54.5 3.5 %all-to-all-start.4 = ((bf16[4,128,512]{1,2,0:T(8,128)(2,1)}), bf16[4,128,512]{1,2,0:T(8,128)(2,1)S(1)}, u32[]{:S(2)}, u32[]{:S(2)}) async-start(bf16[4,128,512]{1,2,0:T(8,128)(2,1)} %copy.23), calls=%async_computation.4 | async-start | bytes 1048576 | tf_op jit(solution)/shard_map/all_to_all | solution.py:54
  58.8 7.9 %all-to-all-done.4 = bf16[4,128,512]{1,2,0:T(8,128)(2,1)S(1)} async-done(((bf16[4,128,512]{1,2,0:T(8,128)(2,1)}), bf16[4,128,512]{1,2,0:T(8,128)(2,1)S(1)}, u32[]{:S(2)}, u32[]{:S(2)}) %all-to-all-start.4) | async-done | bytes 524320 | tf_op jit(solution)/shard_map/all_to_all | solution.py:54
  66.8 4.6 %all-to-all-start.3 = ((bf16[128,4,1,128]{3,0,2,1:T(8,128)(2,1)}), bf16[128,4,1,128]{3,0,2,1:T(8,128)(2,1)S(1)}, u32[]{:S(2)}, u32[]{:S(2)}) async-start(bf16[128,4,1,128]{3,0,2,1:T(8,128)(2,1)} %bitcast.12), calls=%async_computation.3 | async-start | bytes 262144 | tf_op jit(solution)/shard_map/all_to_all | solution.py:83
  71.5 1.0 copy.24
  72.5 4.8 %all-to-all-done.3 = bf16[128,4,1,128]{3,0,2,1:T(8,128)(2,1)S(1)} async-done(((bf16[128,4,1,128]{3,0,2,1:T(8,128)(2,1)}), bf16[128,4,1,128]{3,0,2,1:T(8,128)(2,1)S(1)}, u32[]{:S(2)}, u32[]{:S(2)}) %all-to-all-start.3) | async-done | bytes 131104 | tf_op jit(solution)/shard_map/all_to_all | solution.py:83
  77.3 3.5 %all-to-all-start.5 = ((bf16[128,4,4,128]{3,0,2,1:T(8,128)(2,1)}), bf16[128,4,4,128]{3,0,2,1:T(8,128)(2,1)S(1)}, u32[]{:S(2)}, u32[]{:S(2)}) async-start(bf16[128,4,4,128]{3,0,2,1:T(8,128)(2,1)} %copy.24), calls=%async_computation.5 | async-start | bytes 1048576 | tf_op jit(solution)/shard_map/all_to_all | solution.py:81
  80.9 1.2 reduce-window.6
  82.8 11.1 %all-to-all-done.5 = bf16[128,4,4,128]{3,0,2,1:T(8,128)(2,1)S(1)} async-done(((bf16[128,4,4,128]{3,0,2,1:T(8,128)(2,1)}), bf16[128,4,4,128]{3,0,2,1:T(8,128)(2,1)S(1)}, u32[]{:S(2)}, u32[]{:S(2)}) %all-to-all-start.5) | async-done | bytes 524320 | tf_op jit(solution)/shard_map/all_to_all | solution.py:81
  93.9 3.3 %all-to-all-start.1 = ((bf16[128,4,1,128]{3,0,2,1:T(8,128)(2,1)}), bf16[128,4,1,128]{3,0,2,1:T(8,128)(2,1)S(1)}, u32[]{:S(2)}, u32[]{:S(2)}) async-start(bf16[128,4,1,128]{3,0,2,1:T(8,128)(2,1)} %bitcast.4), calls=%async_computation.1 | async-start | bytes 262144 | tf_op jit(solution)/shard_map/all_to_all | solution.py:84
  97.9 1.3 fusion.3
  99.2 1.9 %copy-done.1 = f32[512,512,4]{1,0,2:T(8,128)} copy-done((f32[512,512,4]{1,0,2:T(8,128)}, f32[512,512,4]{1,0,2:T(8,128)S(1)}, u32[]{:S(2)}) %copy-start.1) | copy-done | bytes 4194328
  101.2 1.4 %fusion.2 = f32[4,512]{1,0:T(4,128)S(1)} fusion(f32[512,512,4]{1,0,2:T(8,128)S(1)} %get-tuple-element.24, f32[4,512]{1,0:T(4,128)S(1)} %get-tuple-element.23, f32[4,512]{1,0:T(4,128)S(1)} %bitcast.171, f32[4]{0:T(128)S(1)} %dynamic-slice_multiply_fusion, pred[512,512]{0,1:T(8,128)(4,1)S(1)} %iota_compare_fusion), kind=kLoop, calls=%fused_computation.6 | loop fusion | flops 6289408 | bytes 4481040 | tf_op jit(solution)/shard_map/while/body/eval_jaxpr/reduce_sum | solution.py:124
  103.1 3.7 %multiply_reduce_fusion = (f32[512,4]{0,1:T(4,128)S(1)}, f32[512,1,4,128]{0,3,2,1:T(8,128)S(1)}) fusion(bf16[512,128,1]{1,0,2:T(8,128)(2,1)S(1)} %bitcast.169, f32[4,512]{1,0:T(4,128)S(1)} %fusion.2, f32[4,512]{1,0:T(4,128)S(1)} %get-tuple-element.23, f32[4,512]{1,0:T(4,128)S(1)} %bitcast.172, f32[4]{0:T(128)S(1)} %dynamic-slice_multiply_fusion, ...), kind=kOutput, calls=%fused_computation.23 | convolution fusion | flops 276297728 | bytes 5668880 | tf_op jit(solution)/shard_map/while/body/eval_jaxpr/kgqs,skd->qkgd/dot_general | solution.py:125
  107.4 17.5 %all_to_all.102 = bf16[512,4,128]{2,1,0:T(4,128)(2,1)S(1)} all-to-all(bf16[512,4,128]{2,1,0:T(4,128)(2,1)S(1)} %copy.27), channel_id=1, replica_groups=mesh['grp'=2,'sp'=4,'dp'=4] {'sp'}, dimensions={0} | all-to-all | bytes 1048576 | tf_op jit(solution)/shard_map/all_to_all | solution.py:132
  125.0 1.2 reshape.234
  (35 shorter events, 6.1 us)
Async XLA Ops:
  6.5 43.3 %copy-start = (bf16[2048,512]{1,0:T(8,128)(2,1)S(1)}, bf16[2048,512]{1,0:T(8,128)(2,1)}, u32[]{:S(2)}) copy-start(bf16[2048,512]{1,0:T(8,128)(2,1)} %param.11) | copy-start | bytes 6291460
  6.5 34.7 %copy-start.2 = (bf16[2048,128]{1,0:T(8,128)(2,1)S(1)}, bf16[2048,128]{1,0:T(8,128)(2,1)}, u32[]{:S(2)}) copy-start(bf16[2048,128]{1,0:T(8,128)(2,1)} %param.12) | copy-start | bytes 1572868
  6.5 27.7 %all-gather.2.cloned.1.call-start = ((), (), s32[]{:S(2)}) async-start(), calls=%async_computation.8 | async-start | bytes 2621440 | tf_op jit(solution)/shard_map/all_gather | solution.py:35
  9.2 28.0 %all-to-all-start.6 = ((bf16[128,4,4]{0,2,1:T(4,128)(2,1)}), bf16[128,4,4]{0,2,1:T(4,128)(2,1)S(1)}, u32[]{:S(2)}, u32[]{:S(2)}) async-start(bf16[128,4,4]{0,2,1:T(4,128)(2,1)} %bitcast.32), calls=%async_computation.6 | async-start | bytes 8192 | tf_op jit(solution)/shard_map/all_to_all | solution.py:82
  37.3 8.6 %all-to-all-start = ((bf16[4,128,128]{2,1,0:T(8,128)(2,1)}), bf16[4,128,128]{2,1,0:T(8,128)(2,1)}, u32[]{:S(2)}, u32[]{:S(2)}) async-start(bf16[4,128,128]{2,1,0:T(8,128)(2,1)} %bitcast.1), calls=%async_computation | async-start | bytes 262144 | tf_op jit(solution)/shard_map/all_to_all | solution.py:56
  45.9 8.6 %all-to-all-start.2 = ((bf16[4,128,128]{2,1,0:T(8,128)(2,1)}), bf16[4,128,128]{2,1,0:T(8,128)(2,1)}, u32[]{:S(2)}, u32[]{:S(2)}) async-start(bf16[4,128,128]{2,1,0:T(8,128)(2,1)} %bitcast.9), calls=%async_computation.2 | async-start | bytes 262144 | tf_op jit(solution)/shard_map/all_to_all | solution.py:55
  49.9 8.1 %copy-start.3 = (f32[16]{0:T(128)S(1)}, f32[16]{0:T(128)}, u32[]{:S(2)}) copy-start(f32[16]{0:T(128)} %param.15) | copy-start | bytes 196
  49.9 21.5 %copy-start.4 = (f32[16]{0:T(128)S(1)}, f32[16]{0:T(128)}, u32[]{:S(2)}) copy-start(f32[16]{0:T(128)} %param.16) | copy-start | bytes 196
  54.5 12.3 %all-to-all-start.4 = ((bf16[4,128,512]{1,2,0:T(8,128)(2,1)}), bf16[4,128,512]{1,2,0:T(8,128)(2,1)S(1)}, u32[]{:S(2)}, u32[]{:S(2)}) async-start(bf16[4,128,512]{1,2,0:T(8,128)(2,1)} %copy.23), calls=%async_computation.4 | async-start | bytes 1048576 | tf_op jit(solution)/shard_map/all_to_all | solution.py:54
  66.8 10.6 %all-to-all-start.3 = ((bf16[128,4,1,128]{3,0,2,1:T(8,128)(2,1)}), bf16[128,4,1,128]{3,0,2,1:T(8,128)(2,1)S(1)}, u32[]{:S(2)}, u32[]{:S(2)}) async-start(bf16[128,4,1,128]{3,0,2,1:T(8,128)(2,1)} %bitcast.12), calls=%async_computation.3 | async-start | bytes 262144 | tf_op jit(solution)/shard_map/all_to_all | solution.py:83
  77.3 16.5 %all-to-all-start.5 = ((bf16[128,4,4,128]{3,0,2,1:T(8,128)(2,1)}), bf16[128,4,4,128]{3,0,2,1:T(8,128)(2,1)S(1)}, u32[]{:S(2)}, u32[]{:S(2)}) async-start(bf16[128,4,4,128]{3,0,2,1:T(8,128)(2,1)} %copy.24), calls=%async_computation.5 | async-start | bytes 1048576 | tf_op jit(solution)/shard_map/all_to_all | solution.py:81
  93.9 9.2 %all-to-all-start.1 = ((bf16[128,4,1,128]{3,0,2,1:T(8,128)(2,1)}), bf16[128,4,1,128]{3,0,2,1:T(8,128)(2,1)S(1)}, u32[]{:S(2)}, u32[]{:S(2)}) async-start(bf16[128,4,1,128]{3,0,2,1:T(8,128)(2,1)} %bitcast.4), calls=%async_computation.1 | async-start | bytes 262144 | tf_op jit(solution)/shard_map/all_to_all | solution.py:84
  99.2 1.9 %copy-start.1 = (f32[512,512,4]{1,0,2:T(8,128)}, f32[512,512,4]{1,0,2:T(8,128)S(1)}, u32[]{:S(2)}) copy-start(f32[512,512,4]{1,0,2:T(8,128)S(1)} %get-tuple-element.24) | copy-start | bytes 12582916
Sparse Core Ops, SparseCore 0:
  8.9 25.2 all-gather.1
where the time goes:
time: 134 us; the launch traced here: 133 us
  waiting for transfers between devices  46.2 us (34%)
  starting transfers between devices  29.1 us (22%)
  blocking collectives  17.5 us (13%)
  matrix products  15.8 us (12%)
  between operations  13.6 us (10%)
  local copies, waits for them, and re-layouts  6.66 us (5%)
  other arithmetic  4.19 us (3%)
    all_gather x1, waiting for transfers between devices, local(): everyone = lax.all_gather(tokens, 'dp', axis=0, tiled=True)  18.6 us
    all_to_all x1, blocking collectives, local(): lax.all_to_all(outputs, 'sp', split_axis=0, concat_axis=1, tiled=True)  17.5 us
    all_to_all x1, waiting for transfers between devices, local(): lax.all_to_all(query_send, 'sp', split_axis=1, concat_axis=0, tiled=True)  11.1 us
    all_to_all x1, waiting for transfers between devices, local(): lax.all_to_all(query_cols, 'dp', split_axis=0, concat_axis=2, tiled=True)  7.92 us
    all_to_all x1, starting transfers between devices, local(): lax.all_to_all(forget_send, 'sp', split_axis=1, concat_axis=0, tiled=True)  6.35 us
    all_to_all x1, waiting for transfers between devices, local(): lax.all_to_all(key_send, 'sp', split_axis=1, concat_axis=0, tiled=True)  4.79 us
    all_to_all x1, starting transfers between devices, local(): lax.all_to_all(key_send, 'sp', split_axis=1, concat_axis=0, tiled=True)  4.6 us
    all_to_all x1, starting transfers between devices, local(): lax.all_to_all(value_cols, 'dp', split_axis=0, concat_axis=2, tiled=True)  3.97 us
  transfers between devices with their start and end apart: 8, of which 7 were waited for; matrix products, arithmetic and copies ran while one was open for 14% of the time, Pallas kernels for 0%

commit v1 on v0

--- a/solution.py
+++ b/solution.py
@@ -32,7 +32,12 @@
     local_heads = head_count // spread
     local_kv = max(1, kv_heads // spread)
     group_size = local_heads // local_kv
-    everyone = lax.all_gather(tokens, "dp", axis=0, tiled=True)
+    ring = [tokens]
+    for hop in range(3):
+        ring.append(lax.ppermute(ring[-1], "dp", [(dev, (dev + 1) % 4) for dev in range(4)]))
+    everyone = jnp.roll(
+        jnp.concatenate(ring[::-1], axis=0), (lax.axis_index("dp") + 1) * ring[0].shape[0], axis=0
+    )
     seq_count = everyone.shape[0]
     flat_rows = everyone.reshape(seq_count * tok_count, everyone.shape[2])
     query_cols = (

time: 134 us -> 127 us (0.948)
  between operations: 13.6 us -> 0.29 us
  local copies, waits for them, and re-layouts: 6.66 us -> 13.8 us
  matrix products: 15.8 us -> 14.1 us
    ppermute x0 -> x3, waiting for transfers between devices: none -> 19.1 us  [local(): lax.ppermute(ring[-1], 'dp', [(dev, (dev + 1) % 4) for dev in range(4)])]
    all_gather x1 -> x0, waiting for transfers between devices: 18.6 us -> none  [local(): everyone = lax.all_gather(tokens, 'dp', axis=0, tiled=True)]
    unnamed x11 -> x24, local copies, waits for them, and re-layouts: 1.96 us -> 8.82 us
    dot_general x1, matrix products: 3.04 us -> 1.37 us  [local(): jnp.dot(flat_rows, v_weight, preferred_element_type=jnp.float32)]
  transfers between devices with their start and end apart: 8 -> 10, of which waited for: 7 -> 9; matrix products, arithmetic and copies ran while one was open for 14% -> 18% of each run, Pallas kernels for 0% -> 0%
where the time goes in v1:
time: 127 us; the launch traced here: 126 us
  waiting for transfers between devices  46 us (36%)
  starting transfers between devices  29.8 us (23%)
  blocking collectives  17.5 us (14%)
  matrix products  14.1 us (11%)
  local copies, waits for them, and re-layouts  13.8 us (11%)
  other arithmetic  4.19 us (3%)
    ppermute x3, waiting for transfers between devices, local(): lax.ppermute(ring[-1], 'dp', [(dev, (dev + 1) % 4) for dev in range(4)])  19.1 us
    all_to_all x1, blocking collectives, local(): lax.all_to_all(outputs, 'sp', split_axis=0, concat_axis=1, tiled=True)  17.5 us
    all_to_all x1, waiting for transfers between devices, local(): lax.all_to_all(query_send, 'sp', split_axis=1, concat_axis=0, tiled=True)  11.1 us
    unnamed x24, local copies, waits for them, and re-layouts  8.82 us
    all_to_all x1, waiting for transfers between devices, local(): lax.all_to_all(query_cols, 'dp', split_axis=0, concat_axis=2, tiled=True)  7.93 us
    all_to_all x1, starting transfers between devices, local(): lax.all_to_all(forget_send, 'sp', split_axis=1, concat_axis=0, tiled=True)  5.65 us
    all_to_all x1, starting transfers between devices, local(): lax.all_to_all(key_send, 'sp', split_axis=1, concat_axis=0, tiled=True)  5.52 us
    all_to_all x1, waiting for transfers between devices, local(): lax.all_to_all(key_send, 'sp', split_axis=1, concat_axis=0, tiled=True)  4.79 us
  transfers between devices with their start and end apart: 10, of which 9 were waited for; matrix products, arithmetic and copies ran while one was open for 18% of the time, Pallas kernels for 0%

profile of v1, /device:TPU:0, one launch (start us, length us, event | category | flops | bytes accessed | tf_op | source)
XLA Modules:
  0.0 125.7 jit_solution(1481247319470795241)
XLA Ops:
  0.5 9.0 %collective-permute-done = bf16[1,128,2048]{2,1,0:T(8,128)(2,1)S(1)} collective-permute-done((bf16[1,128,2048]{2,1,0:T(8,128)(2,1)}, bf16[1,128,2048]{2,1,0:T(8,128)(2,1)S(1)}, u32[]{:S(2)}, u32[]{:S(2)}) %collective-permute-start) | collective-permute-done | bytes 524320 | tf_op jit(solution)/shard_map/ppermute | solution.py:37
  9.5 8.7 %collective-permute-done.1 = bf16[1,128,2048]{2,1,0:T(8,128)(2,1)} collective-permute-done((bf16[1,128,2048]{2,1,0:T(8,128)(2,1)S(1)}, bf16[1,128,2048]{2,1,0:T(8,128)(2,1)}, u32[]{:S(2)}, u32[]{:S(2)}) %collective-permute-start.1) | collective-permute-done | bytes 524320 | tf_op jit(solution)/shard_map/ppermute | solution.py:37
  18.2 1.9 %fusion.10 = bf16[128,16]{0,1:T(8,128)(2,1)} fusion(bf16[2048,16]{0,1:T(8,128)(2,1)} %param.14, bf16[1,128,2048]{2,1,0:T(8,128)(2,1)} %param.9, f32[128]{0:T(128)} %bitcast.174), kind=kOutput, calls=%fused_computation.16 | convolution fusion | flops 8392704 | bytes 594432 | tf_op jit(solution)/shard_map/dot_general | solution.py:67
  20.2 5.7 %all-to-all-start.6 = ((bf16[128,4,4]{0,2,1:T(4,128)(2,1)}), bf16[128,4,4]{0,2,1:T(4,128)(2,1)S(1)}, u32[]{:S(2)}, u32[]{:S(2)}) async-start(bf16[128,4,4]{0,2,1:T(4,128)(2,1)} %bitcast.32), calls=%async_computation.6 | async-start | bytes 8192 | tf_op jit(solution)/shard_map/all_to_all | solution.py:87
  25.8 1.3 %collective-permute-done.2 = bf16[1,128,2048]{2,1,0:T(8,128)(2,1)} collective-permute-done((bf16[1,128,2048]{2,1,0:T(8,128)(2,1)}, bf16[1,128,2048]{2,1,0:T(8,128)(2,1)}, u32[]{:S(2)}, u32[]{:S(2)}) %collective-permute-start.2) | collective-permute-done | bytes 524320 | tf_op jit(solution)/shard_map/ppermute | solution.py:37
  33.0 1.3 %copy-done.1 = bf16[4,128,2048]{2,1,0:T(8,128)(2,1)} copy-done((bf16[4,128,2048]{2,1,0:T(8,128)(2,1)}, bf16[4,128,2048]{2,1,0:T(8,128)(2,1)S(1)}, u32[]{:S(2)}) %copy-start.1) | copy-done | bytes 2097176
  34.4 1.4 %convolution_convert_fusion.2 = bf16[512,128]{1,0:T(8,128)(2,1)} fusion(bf16[512,2048]{1,0:T(8,128)(2,1)S(1)} %bitcast.161, bf16[2048,128]{1,0:T(8,128)(2,1)S(1)} %copy-done.4), kind=kOutput, calls=%fused_computation.14 | convolution fusion | flops 268500992 | bytes 2752512 | tf_op jit(solution)/shard_map/dot_general | solution.py:54
  35.7 3.9 %all-to-all-start = ((bf16[4,128,128]{2,1,0:T(8,128)(2,1)}), bf16[4,128,128]{2,1,0:T(8,128)(2,1)}, u32[]{:S(2)}, u32[]{:S(2)}) async-start(bf16[4,128,128]{2,1,0:T(8,128)(2,1)} %bitcast.1), calls=%async_computation | async-start | bytes 262144 | tf_op jit(solution)/shard_map/all_to_all | solution.py:61
  39.7 3.0 %convolution_convert_fusion.1 = bf16[512,128]{1,0:T(8,128)(2,1)} fusion(bf16[512,2048]{1,0:T(8,128)(2,1)} %bitcast.162, bf16[2048,128]{1,0:T(8,128)(2,1)S(1)} %copy-done.5), kind=kOutput, calls=%fused_computation.13 | convolution fusion | flops 268500992 | bytes 2752512 | tf_op jit(solution)/shard_map/dot_general | solution.py:49
  42.7 1.8 %all-to-all-done = bf16[4,128,128]{2,1,0:T(8,128)(2,1)} async-done(((bf16[4,128,128]{2,1,0:T(8,128)(2,1)}), bf16[4,128,128]{2,1,0:T(8,128)(2,1)}, u32[]{:S(2)}, u32[]{:S(2)}) %all-to-all-start) | async-done | bytes 131104 | tf_op jit(solution)/shard_map/all_to_all | solution.py:61
  44.5 3.9 %all-to-all-start.2 = ((bf16[4,128,128]{2,1,0:T(8,128)(2,1)}), bf16[4,128,128]{2,1,0:T(8,128)(2,1)}, u32[]{:S(2)}, u32[]{:S(2)}) async-start(bf16[4,128,128]{2,1,0:T(8,128)(2,1)} %bitcast.9), calls=%async_computation.2 | async-start | bytes 262144 | tf_op jit(solution)/shard_map/all_to_all | solution.py:60
  48.5 2.8 %convolution_convert_fusion = bf16[512,512]{1,0:T(8,128)(2,1)S(1)} fusion(bf16[512,2048]{1,0:T(8,128)(2,1)} %bitcast.163, bf16[2048,512]{1,0:T(8,128)(2,1)S(1)} %copy-done), kind=kOutput, calls=%fused_computation.12 | convolution fusion | flops 1074003968 | bytes 4718592 | tf_op jit(solution)/shard_map/dot_general | solution.py:44
  53.1 3.5 %all-to-all-start.4 = ((bf16[4,128,512]{1,2,0:T(8,128)(2,1)}), bf16[4,128,512]{1,2,0:T(8,128)(2,1)S(1)}, u32[]{:S(2)}, u32[]{:S(2)}) async-start(bf16[4,128,512]{1,2,0:T(8,128)(2,1)} %copy.23), calls=%async_computation.4 | async-start | bytes 1048576 | tf_op jit(solution)/shard_map/all_to_all | solution.py:59
  57.4 7.9 %all-to-all-done.4 = bf16[4,128,512]{1,2,0:T(8,128)(2,1)S(1)} async-done(((bf16[4,128,512]{1,2,0:T(8,128)(2,1)}), bf16[4,128,512]{1,2,0:T(8,128)(2,1)S(1)}, u32[]{:S(2)}, u32[]{:S(2)}) %all-to-all-start.4) | async-done | bytes 524320 | tf_op jit(solution)/shard_map/all_to_all | solution.py:59
  65.4 5.5 %all-to-all-start.3 = ((bf16[128,4,1,128]{3,0,2,1:T(8,128)(2,1)}), bf16[128,4,1,128]{3,0,2,1:T(8,128)(2,1)S(1)}, u32[]{:S(2)}, u32[]{:S(2)}) async-start(bf16[128,4,1,128]{3,0,2,1:T(8,128)(2,1)} %bitcast.12), calls=%async_computation.3 | async-start | bytes 262144 | tf_op jit(solution)/shard_map/all_to_all | solution.py:88
  72.0 4.8 %all-to-all-done.3 = bf16[128,4,1,128]{3,0,2,1:T(8,128)(2,1)S(1)} async-done(((bf16[128,4,1,128]{3,0,2,1:T(8,128)(2,1)}), bf16[128,4,1,128]{3,0,2,1:T(8,128)(2,1)S(1)}, u32[]{:S(2)}, u32[]{:S(2)}) %all-to-all-start.3) | async-done | bytes 131104 | tf_op jit(solution)/shard_map/all_to_all | solution.py:88
  76.8 3.5 %all-to-all-start.5 = ((bf16[128,4,4,128]{3,0,2,1:T(8,128)(2,1)}), bf16[128,4,4,128]{3,0,2,1:T(8,128)(2,1)S(1)}, u32[]{:S(2)}, u32[]{:S(2)}) async-start(bf16[128,4,4,128]{3,0,2,1:T(8,128)(2,1)} %copy.24), calls=%async_computation.5 | async-start | bytes 1048576 | tf_op jit(solution)/shard_map/all_to_all | solution.py:86
  82.3 11.1 %all-to-all-done.5 = bf16[128,4,4,128]{3,0,2,1:T(8,128)(2,1)S(1)} async-done(((bf16[128,4,4,128]{3,0,2,1:T(8,128)(2,1)}), bf16[128,4,4,128]{3,0,2,1:T(8,128)(2,1)S(1)}, u32[]{:S(2)}, u32[]{:S(2)}) %all-to-all-start.5) | async-done | bytes 524320 | tf_op jit(solution)/shard_map/all_to_all | solution.py:86
  93.4 3.3 %all-to-all-start.1 = ((bf16[128,4,1,128]{3,0,2,1:T(8,128)(2,1)}), bf16[128,4,1,128]{3,0,2,1:T(8,128)(2,1)S(1)}, u32[]{:S(2)}, u32[]{:S(2)}) async-start(bf16[128,4,1,128]{3,0,2,1:T(8,128)(2,1)} %bitcast.4), calls=%async_computation.1 | async-start | bytes 262144 | tf_op jit(solution)/shard_map/all_to_all | solution.py:89
  97.4 1.3 %fusion.3 = (f32[4,512]{1,0:T(4,128)S(1)}, f32[512,512,4]{1,0,2:T(8,128)S(1)}) fusion(f32[4,512]{1,0:T(4,128)S(1)} %bitcast.170, f32[4]{0:T(128)S(1)} %dynamic-slice_multiply_fusion, pred[512,512]{0,1:T(8,128)(4,1)S(1)} %iota_compare_fusion, bf16[512,4,128]{2,0,1:T(8,128)(2,1)S(1)} %bitcast.166, f32[512,1,1,1,1,1,128]{6,0,5,4,3,2,1:T(8,128)S(1)} %bitcast.168, ...), kind=kOutput, calls=%fused_computation.7 | convolution fusion | flops 273807360 | bytes 5261328 | tf_op jit(solution)/shard_map/while/body/eval_jaxpr/qkgd,skd->kgqs/dot_general | solution.py:117
  98.7 1.9 %copy-done.3 = f32[512,512,4]{1,0,2:T(8,128)} copy-done((f32[512,512,4]{1,0,2:T(8,128)}, f32[512,512,4]{1,0,2:T(8,128)S(1)}, u32[]{:S(2)}) %copy-start.3) | copy-done | bytes 4194328
  100.7 1.4 %fusion.2 = f32[4,512]{1,0:T(4,128)S(1)} fusion(f32[512,512,4]{1,0,2:T(8,128)S(1)} %get-tuple-element.24, f32[4,512]{1,0:T(4,128)S(1)} %get-tuple-element.23, f32[4,512]{1,0:T(4,128)S(1)} %bitcast.171, f32[4]{0:T(128)S(1)} %dynamic-slice_multiply_fusion, pred[512,512]{0,1:T(8,128)(4,1)S(1)} %iota_compare_fusion), kind=kLoop, calls=%fused_computation.6 | loop fusion | flops 6289408 | bytes 4481040 | tf_op jit(solution)/shard_map/while/body/eval_jaxpr/reduce_sum | solution.py:129
  102.6 3.7 %multiply_reduce_fusion = (f32[512,4]{0,1:T(4,128)S(1)}, f32[512,1,4,128]{0,3,2,1:T(8,128)S(1)}) fusion(bf16[512,128,1]{1,0,2:T(8,128)(2,1)S(1)} %bitcast.169, f32[4,512]{1,0:T(4,128)S(1)} %fusion.2, f32[4,512]{1,0:T(4,128)S(1)} %get-tuple-element.23, f32[4,512]{1,0:T(4,128)S(1)} %bitcast.172, f32[4]{0:T(128)S(1)} %dynamic-slice_multiply_fusion, ...), kind=kOutput, calls=%fused_computation.23 | convolution fusion | flops 276297728 | bytes 5668880 | tf_op jit(solution)/shard_map/while/body/eval_jaxpr/kgqs,skd->qkgd/dot_general | solution.py:130
  106.9 17.5 %all_to_all.102 = bf16[512,4,128]{2,1,0:T(4,128)(2,1)S(1)} all-to-all(bf16[512,4,128]{2,1,0:T(4,128)(2,1)S(1)} %copy.27), channel_id=1, replica_groups=mesh['grp'=2,'sp'=4,'dp'=4] {'sp'}, dimensions={0} | all-to-all | bytes 1048576 | tf_op jit(solution)/shard_map/all_to_all | solution.py:137
  (53 shorter events, 15.1 us)
Async XLA Ops:
  0.0 48.4 %copy-start = (bf16[2048,512]{1,0:T(8,128)(2,1)S(1)}, bf16[2048,512]{1,0:T(8,128)(2,1)}, u32[]{:S(2)}) copy-start(bf16[2048,512]{1,0:T(8,128)(2,1)} %param.11) | copy-start | bytes 6291460
  0.0 32.7 %copy-start.2 = (bf16[1,128,2048]{2,1,0:T(8,128)(2,1)S(1)}, bf16[1,128,2048]{2,1,0:T(8,128)(2,1)}, u32[]{:S(2)}) copy-start(bf16[1,128,2048]{2,1,0:T(8,128)(2,1)} %param.9) | copy-start | bytes 1572868
  0.0 9.5 %collective-permute-start = (bf16[1,128,2048]{2,1,0:T(8,128)(2,1)}, bf16[1,128,2048]{2,1,0:T(8,128)(2,1)S(1)}, u32[]{:S(2)}, u32[]{:S(2)}) collective-permute-start(bf16[1,128,2048]{2,1,0:T(8,128)(2,1)} %param.9), channel_id=1, source_target_pairs={{0,1},{1,2},{2,3},{3,0},{4,5},{5,6},{6,7},{7,4},{8,9},{9,10},{10,1... | collective-permute-start | bytes 1572872 | tf_op jit(solution)/shard_map/ppermute | solution.py:37
  9.5 8.7 %collective-permute-start.1 = (bf16[1,128,2048]{2,1,0:T(8,128)(2,1)S(1)}, bf16[1,128,2048]{2,1,0:T(8,128)(2,1)}, u32[]{:S(2)}, u32[]{:S(2)}) collective-permute-start(bf16[1,128,2048]{2,1,0:T(8,128)(2,1)S(1)} %collective-permute-done), channel_id=1, source_target_pairs={{0,1},{1,2},{2,3},{3,0},{4,5},{5,6},{6,7},{7,4},{8,9},{9,10},{10,1... | collective-permute-start | bytes 1572872 | tf_op jit(solution)/shard_map/ppermute | solution.py:37
  18.2 8.9 %collective-permute-start.2 = (bf16[1,128,2048]{2,1,0:T(8,128)(2,1)}, bf16[1,128,2048]{2,1,0:T(8,128)(2,1)}, u32[]{:S(2)}, u32[]{:S(2)}) collective-permute-start(bf16[1,128,2048]{2,1,0:T(8,128)(2,1)} %collective-permute-done.1), channel_id=1, source_target_pairs={{0,1},{1,2},{2,3},{3,0},{4,5},{5,6},{6,7},{7,4},{8,9},{9,10},{10,1... | collective-permute-start | bytes 1572872 | tf_op jit(solution)/shard_map/ppermute | solution.py:37
  20.2 15.6 %all-to-all-start.6 = ((bf16[128,4,4]{0,2,1:T(4,128)(2,1)}), bf16[128,4,4]{0,2,1:T(4,128)(2,1)S(1)}, u32[]{:S(2)}, u32[]{:S(2)}) async-start(bf16[128,4,4]{0,2,1:T(4,128)(2,1)} %bitcast.32), calls=%async_computation.6 | async-start | bytes 8192 | tf_op jit(solution)/shard_map/all_to_all | solution.py:87
  30.4 3.9 %copy-start.4 = (bf16[2048,128]{1,0:T(8,128)(2,1)S(1)}, bf16[2048,128]{1,0:T(8,128)(2,1)}, u32[]{:S(2)}) copy-start(bf16[2048,128]{1,0:T(8,128)(2,1)} %param.13) | copy-start | bytes 1572868
  32.7 7.0 %copy-start.5 = (bf16[2048,128]{1,0:T(8,128)(2,1)S(1)}, bf16[2048,128]{1,0:T(8,128)(2,1)}, u32[]{:S(2)}) copy-start(bf16[2048,128]{1,0:T(8,128)(2,1)} %param.12) | copy-start | bytes 1572868
  33.0 1.3 %copy-start.1 = (bf16[4,128,2048]{2,1,0:T(8,128)(2,1)}, bf16[4,128,2048]{2,1,0:T(8,128)(2,1)S(1)}, u32[]{:S(2)}) copy-start(bf16[4,128,2048]{2,1,0:T(8,128)(2,1)S(1)} %constant_dynamic-slice_fusion) | copy-start | bytes 6291460
  35.7 8.7 %all-to-all-start = ((bf16[4,128,128]{2,1,0:T(8,128)(2,1)}), bf16[4,128,128]{2,1,0:T(8,128)(2,1)}, u32[]{:S(2)}, u32[]{:S(2)}) async-start(bf16[4,128,128]{2,1,0:T(8,128)(2,1)} %bitcast.1), calls=%async_computation | async-start | bytes 262144 | tf_op jit(solution)/shard_map/all_to_all | solution.py:61
  44.5 8.6 %all-to-all-start.2 = ((bf16[4,128,128]{2,1,0:T(8,128)(2,1)}), bf16[4,128,128]{2,1,0:T(8,128)(2,1)}, u32[]{:S(2)}, u32[]{:S(2)}) async-start(bf16[4,128,128]{2,1,0:T(8,128)(2,1)} %bitcast.9), calls=%async_computation.2 | async-start | bytes 262144 | tf_op jit(solution)/shard_map/all_to_all | solution.py:60
  48.4 8.1 %copy-start.6 = (f32[16]{0:T(128)S(1)}, f32[16]{0:T(128)}, u32[]{:S(2)}) copy-start(f32[16]{0:T(128)} %param.15) | copy-start | bytes 196
  48.5 22.4 %copy-start.7 = (f32[16]{0:T(128)S(1)}, f32[16]{0:T(128)}, u32[]{:S(2)}) copy-start(f32[16]{0:T(128)} %param.16) | copy-start | bytes 196
  53.1 12.3 %all-to-all-start.4 = ((bf16[4,128,512]{1,2,0:T(8,128)(2,1)}), bf16[4,128,512]{1,2,0:T(8,128)(2,1)S(1)}, u32[]{:S(2)}, u32[]{:S(2)}) async-start(bf16[4,128,512]{1,2,0:T(8,128)(2,1)} %copy.23), calls=%async_computation.4 | async-start | bytes 1048576 | tf_op jit(solution)/shard_map/all_to_all | solution.py:59
  65.4 11.5 %all-to-all-start.3 = ((bf16[128,4,1,128]{3,0,2,1:T(8,128)(2,1)}), bf16[128,4,1,128]{3,0,2,1:T(8,128)(2,1)S(1)}, u32[]{:S(2)}, u32[]{:S(2)}) async-start(bf16[128,4,1,128]{3,0,2,1:T(8,128)(2,1)} %bitcast.12), calls=%async_computation.3 | async-start | bytes 262144 | tf_op jit(solution)/shard_map/all_to_all | solution.py:88
  76.8 16.5 %all-to-all-start.5 = ((bf16[128,4,4,128]{3,0,2,1:T(8,128)(2,1)}), bf16[128,4,4,128]{3,0,2,1:T(8,128)(2,1)S(1)}, u32[]{:S(2)}, u32[]{:S(2)}) async-start(bf16[128,4,4,128]{3,0,2,1:T(8,128)(2,1)} %copy.24), calls=%async_computation.5 | async-start | bytes 1048576 | tf_op jit(solution)/shard_map/all_to_all | solution.py:86
  93.4 9.2 %all-to-all-start.1 = ((bf16[128,4,1,128]{3,0,2,1:T(8,128)(2,1)}), bf16[128,4,1,128]{3,0,2,1:T(8,128)(2,1)S(1)}, u32[]{:S(2)}, u32[]{:S(2)}) async-start(bf16[128,4,1,128]{3,0,2,1:T(8,128)(2,1)} %bitcast.4), calls=%async_computation.1 | async-start | bytes 262144 | tf_op jit(solution)/shard_map/all_to_all | solution.py:89
  98.7 1.9 %copy-start.3 = (f32[512,512,4]{1,0,2:T(8,128)}, f32[512,512,4]{1,0,2:T(8,128)S(1)}, u32[]{:S(2)}) copy-start(f32[512,512,4]{1,0,2:T(8,128)S(1)} %get-tuple-element.24) | copy-start | bytes 12582916
